TPU v7x, 256 devices: a whole 4x4x8 slice. The times are simulated.
256 devices in a mesh: ep: 128 (over z, y, x), tp: 2 (over core).
Axes of the slice: x: 4, y: 4, z: 8, core: 2. Of those that a mesh axis runs over, the one named last changes fastest.
Arguments:
- tokens: bfloat16 [2048, 1024], P('ep'), may hold values from -6 to 6
- lengths: int32 [2048], P('ep'), may hold values from 1 to 1024, 1048576 in all
- routes: int32 [2048, 2], replicated, may hold values from 0 to 15, all different within a row; in each aligned block of 16 rows (0 to 15, 16 to 31, ...) at most 4 rows name the same one
- route_weights: float32 [2048, 2], replicated, may hold values from 0.1 to 1
- key_cache: bfloat16 [2048, 1024, 256], P('ep', None, 'tp'), may hold values from -6 to 6
- value_cache: bfloat16 [2048, 1024, 256], P('ep', None, 'tp'), may hold values from -6 to 6
- w_query: bfloat16 [1024, 1024], P(None, 'tp'), may hold values from -0.1875 to 0.1875
- w_key: bfloat16 [1024, 256], P(None, 'tp'), may hold values from -0.1875 to 0.1875
- w_value: bfloat16 [1024, 256], P(None, 'tp'), may hold values from -0.1875 to 0.1875
- w_out: bfloat16 [1024, 1024], P('tp'), may hold values from -0.1875 to 0.1875
- score_offset: float32 [16], P('tp'), may hold values from -9 to -3
- attn_gain: float32 [1024], replicated, may hold values from 0.1 to 1.9
- ffn_gain: float32 [1024], replicated, may hold values from 0.1 to 1.9
- w_gate: bfloat16 [1024, 114688], P(None, ('ep', 'tp')), may hold values from -0.1875 to 0.1875
- w_up: bfloat16 [1024, 114688], P(None, ('ep', 'tp')), may hold values from -0.1875 to 0.1875
- w_down: bfloat16 [114688, 1024], P(('ep', 'tp')), may hold values from -0.0625 to 0.0625
Outputs:
- layer_out: bfloat16 [2048, 1024], P('ep', 'tp')
- new_keys: bfloat16 [2048, 256], P('ep', 'tp')
- new_values: bfloat16 [2048, 256], P('ep', 'tp')
Inputs may be any that keep to these rules, and one draw needn't show every extreme that they name: `routes`: each row names 2 different experts. Among the rows of one index of ep (aligned blocks of 16 rows) no expert is named by more than 4 rows, and in some block one expert is named by exactly 4 rows.
All inputs are finite; a program needn't handle non-finite values. No bound on the sum of `lengths` on one device may be relied on, other than what follows from the above.
Results may differ from a plain program's by a relative error of at most 0.0095.
Values may be sent and summed in bfloat16 or wider, within the bound.
A program may use at most 128 MiB of HBM per device.

v0:
```python
import math

import jax
import jax.numpy as jnp
from jax import lax
from jax.sharding import PartitionSpec as P

HEAD_DIM = 64
EXPERTS = 16


norm_eps = 1e-06


def total_of_pieces(x, axis):
    parts = lax.all_gather(x, axis).astype(jnp.float32)
    return parts.sum(axis=0)


def cut_along(x, dim, devices):
    dims = x.shape
    parts = x.reshape(*dims[:dim], devices, dims[dim] // devices, *dims[dim + 1 :])
    return jnp.moveaxis(parts, dim, 0)


def summed_on_arrival(x, axis, dim):
    devices = lax.axis_size(axis)
    parts = lax.all_to_all(cut_along(x, dim, devices), axis, 0, 0, tiled=True)
    return jnp.sum(parts.astype(jnp.float32), axis=0)


def rms_rows(values, gain_row):
    widened = values.astype(jnp.float32)
    scaled = widened * lax.rsqrt(jnp.mean(widened * widened, axis=-1, keepdims=True) + norm_eps)
    return (scaled * gain_row).astype(jnp.bfloat16)


def expert_rows(inputs, gate_cols, up_cols, down_rows):
    gate = jnp.dot(inputs, gate_cols, preferred_element_type=jnp.float32)
    upward = jnp.dot(inputs, up_cols, preferred_element_type=jnp.float32)
    hidden = (jax.nn.silu(gate) * upward).astype(jnp.bfloat16)
    return jnp.dot(hidden, down_rows, preferred_element_type=jnp.float32)


def later_sums(log_fail):
    dims_shape = log_fail.shape
    context = dims_shape[-1]
    span_width = math.gcd(context, 128)
    block_count = context // span_width
    blocks = log_fail.reshape(dims_shape[:-1] + (block_count, span_width))
    position_ids = jnp.arange(span_width, dtype=jnp.int32)
    inside_mask = (position_ids[:, None] > position_ids[None, :]).astype(jnp.float32)
    within = jnp.einsum("...cw,wv->...cv", blocks, inside_mask)
    totals = jnp.sum(blocks, axis=-1)
    block_ids = jnp.arange(block_count, dtype=jnp.int32)
    across_mask = (block_ids[:, None] > block_ids[None, :]).astype(jnp.float32)
    carried = jnp.einsum("...c,cb->...b", totals, across_mask)
    return (within + carried[..., None]).reshape(dims_shape)


def code_slots(expert_ids, capacity):
    onehot = (expert_ids[..., None] == jnp.arange(EXPERTS, dtype=jnp.int32)).astype(jnp.int32)
    before = jnp.cumsum(onehot, axis=-2) - onehot
    slot_index = jnp.sum(before * onehot, axis=-1)
    return expert_ids * capacity + slot_index


def shards(
    tokens,
    lengths,
    routes,
    route_weights,
    key_cache,
    value_cache,
    w_query,
    w_key,
    w_value,
    w_out,
    score_offset,
    attn_gain,
    ffn_gain,
    w_gate,
    w_up,
    w_down,
):
    seq_count = tokens.shape[0]
    model_width = tokens.shape[1]
    context = key_cache.shape[1]
    kv_local = key_cache.shape[2] // HEAD_DIM
    heads_local = w_query.shape[1] // HEAD_DIM
    group_size = heads_local // kv_local
    normed = rms_rows(tokens, attn_gain)
    queries = jnp.dot(normed, w_query, preferred_element_type=jnp.float32).astype(jnp.bfloat16)
    new_keys = jnp.dot(normed, w_key, preferred_element_type=jnp.float32).astype(jnp.bfloat16)
    new_values = jnp.dot(normed, w_value, preferred_element_type=jnp.float32).astype(jnp.bfloat16)
    query_heads = queries.reshape(seq_count, kv_local, group_size, HEAD_DIM)
    cache_keys = key_cache.reshape(seq_count, context, kv_local, HEAD_DIM)
    cache_values = value_cache.reshape(seq_count, context, kv_local, HEAD_DIM)
    scores = jnp.einsum(
        "bkgd,bskd->bkgs", query_heads, cache_keys, preferred_element_type=jnp.float32
    )
    scores = (
        scores * HEAD_DIM ** (-0.5) + score_offset.reshape(kv_local, group_size)[None, :, :, None]
    )
    valid = jnp.arange(context, dtype=jnp.int32)[None, None, None, :] < lengths[:, None, None, None]
    log_fail = jnp.where(valid, jax.nn.log_sigmoid(-scores), 0.0)
    after = later_sums(log_fail)
    stick = jnp.where(valid, jnp.exp(jax.nn.log_sigmoid(scores) + after), 0.0).astype(jnp.bfloat16)
    attended = jnp.einsum(
        "bkgs,bskd->bkgd", stick, cache_values, preferred_element_type=jnp.float32
    )
    attended = attended.astype(jnp.bfloat16).reshape(seq_count, heads_local * HEAD_DIM)
    partial_part = jnp.dot(attended, w_out, preferred_element_type=jnp.float32)
    middle = (
        tokens.astype(jnp.float32)
        + total_of_pieces(partial_part.astype(jnp.bfloat16), "tp").astype(jnp.float32)
    ).astype(jnp.bfloat16)
    moe_in = rms_rows(middle, ffn_gain)
    top_count = routes.shape[1]
    capacity = max(2, 2 * seq_count * top_count // EXPERTS)
    sources = lax.axis_size("ep")
    span_size = sources // EXPERTS
    half_width = model_width // lax.axis_size("tp")
    ep_index = lax.axis_index("ep")
    tp_index = lax.axis_index("tp")
    own_routes = lax.dynamic_slice_in_dim(routes, ep_index * seq_count, seq_count, 0)
    own_weights = lax.dynamic_slice_in_dim(route_weights, ep_index * seq_count, seq_count, 0)
    own_codes = code_slots(own_routes.reshape(-1), capacity)
    slot_range = jnp.arange(EXPERTS * capacity, dtype=jnp.int32)
    picker = (slot_range[:, None] == own_codes[None, :]).astype(jnp.bfloat16)
    spread = jnp.repeat(moe_in, top_count, axis=0)
    outgoing = jnp.dot(picker, spread, preferred_element_type=jnp.float32).astype(jnp.bfloat16)
    outgoing = jnp.repeat(outgoing.reshape(EXPERTS, capacity, model_width), span_size, axis=0)
    arrived = lax.all_to_all(outgoing, "ep", split_axis=0, concat_axis=0, tiled=True)
    slot_count = arrived.shape[1]
    expert_term = expert_rows(arrived.reshape(-1, model_width), w_gate, w_up, w_down)
    expert_term = expert_term.reshape(sources, slot_count, model_width)
    shares = summed_on_arrival(expert_term.astype(jnp.bfloat16), "tp", 2)
    returned = lax.all_to_all(
        shares.astype(jnp.bfloat16), "ep", split_axis=0, concat_axis=0, tiled=True
    ).astype(shares.dtype)
    results = jnp.sum(returned.reshape(EXPERTS, span_size, capacity, half_width), axis=1)
    results = results.reshape(EXPERTS * capacity, half_width)
    matched = slot_range[None, None, :] == own_codes.reshape(seq_count, top_count)[:, :, None]
    weighted = jnp.sum(jnp.where(matched, own_weights[:, :, None], 0.0), axis=1)
    mixture = jnp.dot(weighted, results)
    own_middle = lax.dynamic_slice_in_dim(middle, tp_index * half_width, half_width, 1)
    layer_out = (own_middle.astype(jnp.float32) + mixture).astype(jnp.bfloat16)
    return (layer_out, new_keys, new_values)


def solution(mesh):
    in_specs = (
        P("ep", None),
        P("ep"),
        P(),
        P(),
        P("ep", None, "tp"),
        P("ep", None, "tp"),
        P(None, "tp"),
        P(None, "tp"),
        P(None, "tp"),
        P("tp", None),
        P("tp"),
        P(),
        P(),
        P(None, ("ep", "tp")),
        P(None, ("ep", "tp")),
        P(("ep", "tp"), None),
    )
    out_specs = (P("ep", "tp"), P("ep", "tp"), P("ep", "tp"))
    return jax.shard_map(shards, mesh=mesh, in_specs=in_specs, out_specs=out_specs, check_vma=False)
```

profile of v0, /device:TPU:1, one launch (start us, length us, event | category | flops | bytes accessed | tf_op | source)
XLA Modules:
  0.0 118.8 jit_solution(5837329286921709950)
XLA Ops:
  0.7 0.8 constant_dynamic-slice_fusion.1
  1.5 0.1 copy.63
  1.6 0.1 eq.42
  1.7 0.1 fusion.31
  1.7 0.1 reduce_window_sum.11
  1.8 0.2 select_reduce_fusion.1
  2.0 0.9 fusion.22
  2.9 1.6 %convolution_convert_fusion.4 = bf16[16,512]{1,0:T(8,128)(2,1)S(1)} fusion(bf16[1024,512]{1,0:T(8,128)(2,1)} %param.22, bf16[16,1024]{1,0:T(8,128)(2,1)} %param.16, f32[1024]{0:T(1024)} %param.27, f32[16]{0:T(128)S(1)} %add_rsqrt_fusion.1), kind=kOutput, calls=%fused_computation.13 | convolution fusion | flops 16850944 | bytes 1101888 | tf_op jit(solution)/shard_map/dot_general | solution.py:93
  4.4 0.1 reshape.107
  4.5 0.7 iota_compare_fusion.1
  5.3 6.4 %copy.51 = bf16[16,1024,128]{1,2,0:T(8,128)(2,1)} copy(bf16[16,1024,128]{2,1,0:T(8,128)(2,1)} %param.20) | data formatting | bytes 8388608 | tf_op args[4]
  11.7 0.1 add.74
  11.8 3.2 %fusion.14 = (f32[16,2,4,1024]{3,2,1,0:T(4,128)S(1)}, f32[16,2,4,1024]{3,2,1,0:T(4,128)S(1)}) fusion(pred[16,1024]{1,0:T(8,128)(4,1)S(1)} %iota_compare_fusion.1, f32[2,4]{1,0:T(2,128)S(1)} %add.74, bf16[16,2,4,64]{3,2,1,0:T(4,128)(2,1)S(1)} %reshape.107, bf16[16,1024,2,64]{1,3,2,0:T(8,128)(2,1)} %bitcast.40), kind=kOutput, calls=%fused_computation.29 | convolution fusion | flops 18087936 | bytes 5275680 | tf_op jit(solution)/shard_map/bkgd,bskd->bkgs/dot_general | solution.py:99
  15.0 0.2 reshape.109
  15.2 0.3 reduce_sum.78
  15.5 0.2 fusion.26
  15.7 0.1 copy.53
  15.8 0.2 convolution_add_fusion
  16.1 0.2 reshape.110
  16.2 6.4 %copy.54 = bf16[16,1024,128]{1,2,0:T(8,128)(2,1)} copy(bf16[16,1024,128]{2,1,0:T(8,128)(2,1)} %param.21) | data formatting | bytes 8388608 | tf_op args[5]
  22.7 3.4 %convolution_convert_fusion.3 = bf16[16,2,4,64]{3,2,1,0:T(4,128)(2,1)S(1)} fusion(bf16[16,1024,2,64]{1,3,2,0:T(8,128)(2,1)} %bitcast.41, f32[16,2,4,1024]{3,2,1,0:T(4,128)S(1)} %reshape.110, f32[16,2,4,1024]{3,2,1,0:T(4,128)S(1)} %get-tuple-element.6, pred[16,1024]{1,0:T(8,128)(4,1)S(1)} %iota_compare_fusion.1), kind=kOutput, calls=%fused_computation.10 | convolution fusion | flops 18227200 | bytes 5275648 | tf_op jit(solution)/shard_map/bkgs,bskd->bkgd/dot_general | solution.py:109
  26.1 0.1 reshape.112
  26.2 0.2 convolution_convert_fusion.2
  26.4 4.7 %all-gather = bf16[32,1024]{1,0:T(8,128)(2,1)S(1)} all-gather(bf16[16,1024]{1,0:T(8,128)(2,1)S(1)} %convolution_convert_fusion.2), channel_id=2, replica_groups=mesh['ep'=128,'tp'=2] {'tp'}, dimensions={0}, use_global_device_ids=true | all-gather | bytes 98304 | tf_op jit(solution)/shard_map/all_gather | solution.py:16
  31.1 0.1 fusion.19
  31.3 0.1 fusion.21
  31.4 0.2 convolution_convert_fusion.1
  31.6 0.1 reshape.114
  31.7 0.3 broadcast_in_dim.52
  32.0 42.8 %all_to_all.15 = bf16[128,4,1024]{2,1,0:T(4,128)(2,1)S(1)} all-to-all(bf16[128,4,1024]{2,1,0:T(4,128)(2,1)S(1)} %bitcast.42), channel_id=1, replica_groups=mesh['ep'=128,'tp'=2] {'ep'}, dimensions={0} | all-to-all | bytes 2097152 | tf_op jit(solution)/shard_map/all_to_all | solution.py:134
  74.7 0.3 reshape.116
  75.0 1.9 %fusion.40 = f32[512,448]{0,1:T(8,128)S(1)} fusion(bf16[512,1024]{1,0:T(8,128)(2,1)S(1)} %reshape.116, bf16[1024,448]{0,1:T(8,128)(2,1)} %param.29), kind=kOutput, calls=%fused_computation.68 | convolution fusion | flops 469762048 | bytes 2883584 | tf_op jit(solution)/shard_map/dot_general | solution.py:39
  76.9 3.8 %convolution_convert_fusion = bf16[512,1024]{1,0:T(8,128)(2,1)} fusion(bf16[448,1024]{1,0:T(8,128)(2,1)} %param.31, bf16[512,1024]{1,0:T(8,128)(2,1)S(1)} %reshape.116, bf16[1024,448]{0,1:T(8,128)(2,1)} %param.30, f32[512,448]{0,1:T(8,128)S(1)} %fusion.40), kind=kOutput, calls=%fused_computation.2 | convolution fusion | flops 941424640 | bytes 4849664 | tf_op jit(solution)/shard_map/dot_general | solution.py:42
  80.7 1.9 %convert_element_type.80 = bf16[128,4,2,512]{3,2,1,0:T(2,128)(2,1)S(1)} reshape(bf16[512,1024]{1,0:T(8,128)(2,1)} %convolution_convert_fusion) | data formatting | bytes 2097152 | tf_op jit(solution)/shard_map/convert_element_type | solution.py:138
  82.6 0.4 copy.68
  83.0 7.2 %all_to_all.16 = bf16[2,128,4,512]{3,2,1,0:T(4,128)(2,1)S(1)} all-to-all(bf16[2,128,4,512]{3,2,1,0:T(4,128)(2,1)S(1)} %bitcast.43), channel_id=1, replica_groups=mesh['ep'=128,'tp'=2] {'tp'}, dimensions={0} | all-to-all | bytes 2097152 | tf_op jit(solution)/shard_map/all_to_all | solution.py:28
  90.3 1.9 %reduce_sum.84 = bf16[128,4,512]{2,1,0:T(4,128)(2,1)} reduce(bf16[2,128,4,512]{3,2,1,0:T(4,128)(2,1)S(1)} %all_to_all.16, bf16[]{:T(256)} %constant.42.clone.1), dimensions={0}, to_apply=%region_7.8 | reduce | flops 262144 | bytes 1572866 | tf_op jit(solution)/shard_map/reduce_sum | solution.py:29
  92.2 6.2 %all-to-all-start.2 = ((bf16[128,4,512]{2,1,0:T(4,128)(2,1)}), bf16[128,4,512]{2,1,0:T(4,128)(2,1)S(1)}, u32[]{:S(2)}, u32[]{:S(2)}) async-start(bf16[128,4,512]{2,1,0:T(4,128)(2,1)} %reduce_sum.84), calls=%async_computation.2 | async-start | bytes 1048576 | tf_op jit(solution)/shard_map/all_to_all | solution.py:139
  98.3 0.1 reduce_sum.81
  98.4 0.1 copy.56
  98.5 0.8 constant_dynamic-slice_fusion
  99.3 0.1 select_reduce_fusion
  99.4 0.8 convolution_convert_fusion.5
  100.2 0.8 convolution_convert_fusion.6
  101.0 16.5 %all-to-all-done.2 = bf16[128,4,512]{2,1,0:T(4,128)(2,1)S(1)} async-done(((bf16[128,4,512]{2,1,0:T(4,128)(2,1)}), bf16[128,4,512]{2,1,0:T(4,128)(2,1)S(1)}, u32[]{:S(2)}, u32[]{:S(2)}) %all-to-all-start.2) | async-done | bytes 524320 | tf_op jit(solution)/shard_map/all_to_all | solution.py:139
  117.5 0.4 convert_reduce_fusion
  117.9 0.1 copy.62
  118.0 0.7 fusion.2
  (22 shorter events, 0.2 us)
Async XLA Ops:
  0.6 25.5 %copy-start = (bf16[512,1024]{1,0:T(8,128)(2,1)S(1)}, bf16[512,1024]{1,0:T(8,128)(2,1)}, u32[]{:S(2)}) copy-start(bf16[512,1024]{1,0:T(8,128)(2,1)} %param.25) | copy-start | bytes 3145732
  5.3 6.4 %copy-start.6 = (f32[8]{0:T(128)S(1)}, f32[8]{0:T(128)}, u32[]{:S(2)}) copy-start(f32[8]{0:T(128)} %param.26) | copy-start | bytes 100
  22.6 8.5 %copy-start.1 = (bf16[16,1024]{1,0:T(8,128)(2,1)S(1)}, bf16[16,1024]{1,0:T(8,128)(2,1)}, u32[]{:S(2)}) copy-start(bf16[16,1024]{1,0:T(8,128)(2,1)} %param.16) | copy-start | bytes 98308
  22.6 8.6 %copy-start.3 = (f32[1024]{0:T(1024)S(1)}, f32[1024]{0:T(1024)}, u32[]{:S(2)}) copy-start(f32[1024]{0:T(1024)} %param.28) | copy-start | bytes 12292
  80.7 18.7 %copy-start.2 = (f32[1024]{0:T(1024)S(1)}, f32[1024]{0:T(1024)}, u32[]{:S(2)}) copy-start(f32[1024]{0:T(1024)} %param.27) | copy-start | bytes 12292
  80.7 18.7 %copy-start.4 = (bf16[1024,128]{1,0:T(8,128)(2,1)S(1)}, bf16[1024,128]{1,0:T(8,128)(2,1)}, u32[]{:S(2)}) copy-start(bf16[1024,128]{1,0:T(8,128)(2,1)} %param.24) | copy-start | bytes 786436
  80.7 19.5 %copy-start.5 = (bf16[1024,128]{1,0:T(8,128)(2,1)S(1)}, bf16[1024,128]{1,0:T(8,128)(2,1)}, u32[]{:S(2)}) copy-start(bf16[1024,128]{1,0:T(8,128)(2,1)} %param.23) | copy-start | bytes 786436
  92.2 25.4 %all-to-all-start.2 = ((bf16[128,4,512]{2,1,0:T(4,128)(2,1)}), bf16[128,4,512]{2,1,0:T(4,128)(2,1)S(1)}, u32[]{:S(2)}, u32[]{:S(2)}) async-start(bf16[128,4,512]{2,1,0:T(4,128)(2,1)} %reduce_sum.84), calls=%async_computation.2 | async-start | bytes 1048576 | tf_op jit(solution)/shard_map/all_to_all | solution.py:139
where the time goes:
time: 119 us
  blocking collectives  54.7 us (46%)
  local copies, waits for them, and re-layouts  18.7 us (16%)
  matrix products  17 us (14%)
  waiting for transfers between devices  16.5 us (14%)
  starting transfers between devices  6.17 us (5%)
  other arithmetic  4.81 us (4%)
    all_to_all x1, blocking collectives, shards(): lax.all_to_all(outgoing, 'ep', split_axis=0, concat_axis=0, tiled=True)  42.8 us
    all_to_all x1, waiting for transfers between devices, shards(): lax.all_to_all(shares.astype(jnp.bfloat16), 'ep', split_axis=0, concat_ax...  16.5 us
    unnamed x18, local copies, waits for them, and re-layouts  13 us
    all_to_all x1, blocking collectives, summed_on_arrival(): parts = lax.all_to_all(cut_along(x, dim, devices), axis, 0, 0, tiled=True)  7.25 us
    all_to_all x1, starting transfers between devices, shards(): lax.all_to_all(shares.astype(jnp.bfloat16), 'ep', split_axis=0, concat_ax...  6.17 us
    all_gather x1, blocking collectives, total_of_pieces(): parts = lax.all_gather(x, axis).astype(jnp.float32)  4.7 us
    dot_general x1, matrix products, expert_rows(): return jnp.dot(hidden, down_rows, preferred_element_type=jnp.float32)  3.82 us
    dot_general x1, matrix products, shards(): jnp.einsum('bkgs,bskd->bkgd', stick, cache_values, preferred_element_type...  3.4 us
  transfers between devices with their start and end apart: 1, of which 1 were waited for; matrix products, arithmetic and copies ran while one was open for 2% of the time, Pallas kernels for 0%

commit v1 on v0

v1 whole, which is shorter than its diff:
```python
import jax
import jax.numpy as jnp
from jax import lax
from jax.experimental import pallas as pl
from jax.experimental.pallas import tpu as pltpu
from jax.sharding import PartitionSpec as P

HEAD_DIM = 64
SEQS = 16
CTX = 1024
HEADS = 8
BLOCK = 256
EPS = 1e-06
MESH = pl.DeviceIdType.MESH
F32 = jnp.float32
BF16 = jnp.bfloat16
HBM = pltpu.HBM
VMEM = pltpu.VMEM


def rms_rows(values, gain_row):
    scaled = values * lax.rsqrt(jnp.mean(values * values, axis=-1, keepdims=True) + EPS)
    return (scaled * gain_row).astype(BF16)


def dot(a, b):
    return jnp.dot(a, b, preferred_element_type=F32)


def dot_nt(a, b):
    return lax.dot_general(a, b, (((1,), (1,)), ((), ())), preferred_element_type=F32)


def iota(shape, dim):
    return lax.broadcasted_iota(jnp.int32, shape, dim)


def attend_kernel(
    tokens_hbm,
    gain_hbm,
    lengths_hbm,
    offset_hbm,
    routes_hbm,
    rweights_hbm,
    keys_hbm,
    values_hbm,
    wq_hbm,
    wk_hbm,
    wv_hbm,
    wo_hbm,
    part_ref,
    new_keys_ref,
    new_values_ref,
    pick_ref,
    weight_ref,
    tokens,
    gain,
    lengths,
    offset,
    routes,
    rweights,
    keys,
    values,
    wq,
    wk,
    wv,
    wo,
    turned,
    small_sem,
    weight_sem,
    key_sem,
    value_sem,
):
    ep = lax.axis_index("ep")
    lane_block = pl.multiple_of((ep // 8) * 128, 128)
    small = [
        pltpu.make_async_copy(tokens_hbm, tokens, small_sem.at[0]),
        pltpu.make_async_copy(gain_hbm, gain, small_sem.at[1]),
        pltpu.make_async_copy(lengths_hbm, lengths, small_sem.at[2]),
        pltpu.make_async_copy(offset_hbm, offset, small_sem.at[3]),
        pltpu.make_async_copy(routes_hbm.at[:, pl.ds(lane_block, 128)], routes, small_sem.at[4]),
        pltpu.make_async_copy(rweights_hbm.at[:, pl.ds(lane_block, 128)], rweights, small_sem.at[5]),
    ]
    weights = [
        pltpu.make_async_copy(wq_hbm, wq, weight_sem.at[0]),
        pltpu.make_async_copy(wk_hbm, wk, weight_sem.at[1]),
        pltpu.make_async_copy(wv_hbm, wv, weight_sem.at[2]),
        pltpu.make_async_copy(wo_hbm, wo, weight_sem.at[3]),
    ]
    key_copies = [
        pltpu.make_async_copy(keys_hbm.at[pl.ds(2 * p, 2)], keys.at[pl.ds(2 * p, 2)], key_sem.at[p])
        for p in range(8)
    ]
    value_copies = [
        pltpu.make_async_copy(values_hbm.at[pl.ds(2 * p, 2)], values.at[pl.ds(2 * p, 2)], value_sem.at[p])
        for p in range(8)
    ]
    for copy in small[:2] + weights[:1] + small[2:] + key_copies + weights[1:3] + value_copies + weights[3:]:
        copy.start()

    for copy in small[4:]:
        copy.wait()
    row = iota((128, 128), 0)
    lane = iota((128, 128), 1)
    mine = (lane // 16) == (ep % 8)
    first = jnp.logical_and(routes[0:1, :] == row // 8, mine)
    second = jnp.logical_and(routes[1:2, :] == row // 8, mine)
    named = jnp.logical_or(first, second)
    earlier = dot(named.astype(F32).astype(BF16), (row < lane).astype(F32).astype(BF16))
    chosen = jnp.logical_and(named, earlier == (row % 4).astype(F32))
    pick_ref[...] = chosen.astype(F32).astype(BF16)
    share = jnp.where(first, rweights[0:1, :], rweights[1:2, :])
    turned[...] = jnp.transpose(jnp.where(chosen, share, 0.0))
    weight_ref[...] = turned[pl.ds(pl.multiple_of((ep % 8) * 16, 16), 16), :]

    small[0].wait()
    small[1].wait()
    normed = rms_rows(tokens[...].astype(F32), gain[...])
    weights[0].wait()
    queries = dot(normed, wq[...])
    low = iota((SEQS, 128), 1) < HEAD_DIM
    by_head = []
    for h in range(HEADS):
        tile = queries[:, 128 * (h // 2) : 128 * (h // 2) + 128]
        if h % 2 != h // 4:
            tile = pltpu.roll(tile, HEAD_DIM, 1)
        by_head.append(jnp.where(low if h < 4 else jnp.logical_not(low), tile, 0.0))
    by_head = jnp.concatenate(by_head, axis=0).astype(BF16)
    to_seq = jnp.logical_and(row // 8 == lane % 16, row % 8 == lane // 16).astype(F32).astype(BF16)
    to_head = jnp.logical_and(row // 16 == lane % 8, row % 16 == lane // 8).astype(F32).astype(BF16)
    by_seq = dot(to_seq, by_head)
    wide = []
    for p in range(8):
        left = jnp.where(row // 8 == 2 * p, by_seq, 0.0).astype(BF16)
        right = jnp.where(row // 8 == 2 * p + 1, by_seq, 0.0).astype(BF16)
        wide.append(jnp.concatenate([left, right], axis=1))

    small[2].wait()
    small[3].wait()
    lane1 = iota((1, 128), 1)
    limit = jnp.zeros((1, 128), jnp.int32)
    for b in range(SEQS):
        limit = jnp.where(lane1 // 8 == b, lengths[b], limit)
    shift = jnp.zeros((1, 128), F32)
    for h in range(HEADS):
        shift = jnp.where(lane1 % 8 == h, offset[h], shift)

    upper = (iota((BLOCK, BLOCK), 1) >= iota((BLOCK, BLOCK), 0)).astype(F32).astype(BF16)
    for copy in key_copies:
        copy.wait()
    carry = jnp.zeros((1, 128), F32)
    sticks = [None] * (CTX // BLOCK)
    for i in reversed(range(CTX // BLOCK)):
        rows = slice(i * BLOCK, (i + 1) * BLOCK)
        scores = jnp.zeros((BLOCK, 128), F32)
        for p in range(8):
            pair = jnp.concatenate([keys[2 * p, rows, :], keys[2 * p + 1, rows, :]], axis=1)
            scores = scores + dot_nt(pair, wide[p])
        z = scores * HEAD_DIM ** (-0.5) + shift
        valid = iota((BLOCK, 128), 0) + i * BLOCK < limit
        fail = jnp.where(valid, -(jnp.maximum(z, 0.0) + jnp.log1p(jnp.exp(-jnp.abs(z)))), 0.0)
        high = fail.astype(BF16)
        rest = (fail - high.astype(F32)).astype(BF16)
        total = dot(upper, high) + dot(upper, rest) + carry
        carry = total[0:1, :]
        stick = jnp.where(valid, jnp.exp(z + total), 0.0)
        sticks[i] = jnp.transpose(stick).astype(BF16)

    weights[1].wait()
    new_keys_ref[...] = dot(normed, wk[...]).astype(BF16)
    weights[2].wait()
    new_values_ref[...] = dot(normed, wv[...]).astype(BF16)

    gathered = []
    top = iota((16, 128), 0) < 8
    for p in range(8):
        value_copies[p].wait()
        both = jnp.zeros((16, 256), F32)
        for i in range(CTX // BLOCK):
            rows = slice(i * BLOCK, (i + 1) * BLOCK)
            pair = jnp.concatenate([values[2 * p, rows, :], values[2 * p + 1, rows, :]], axis=1)
            both = both + dot(sticks[i][16 * p : 16 * p + 16, :], pair)
        gathered.append(jnp.where(top, both[:, :128], both[:, 128:]))
    gathered = jnp.concatenate(gathered, axis=0).astype(BF16)
    gathered = dot(to_head, gathered)
    tiles = []
    for p in range(4):
        pieces = []
        for h in (2 * p, 2 * p + 1):
            piece = gathered[16 * h : 16 * h + 16, :]
            if h % 2 != h // 4:
                piece = pltpu.roll(piece, HEAD_DIM, 1)
            pieces.append(piece)
        tiles.append(jnp.where(low, pieces[0], pieces[1]))
    attended = jnp.concatenate(tiles, axis=1).astype(BF16)
    weights[3].wait()
    part_ref[...] = dot(attended, wo[...]).astype(BF16)


def attend(tokens, lengths, routes, route_weights, key_cache, value_cache, wq, wk, wv, wo, offset, gain):
    hbm = pl.BlockSpec(memory_space=HBM)
    vmem = pl.BlockSpec(memory_space=VMEM)
    return pl.pallas_call(
        attend_kernel,
        name="attend",
        out_shape=(
            jax.ShapeDtypeStruct((SEQS, 1024), BF16),
            jax.ShapeDtypeStruct((SEQS, 128), BF16),
            jax.ShapeDtypeStruct((SEQS, 128), BF16),
            jax.ShapeDtypeStruct((128, 128), BF16),
            jax.ShapeDtypeStruct((16, 128), F32),
        ),
        in_specs=[hbm] * 12,
        out_specs=[vmem] * 5,
        scratch_shapes=[
            VMEM((SEQS, 1024), BF16),
            VMEM((1, 1024), F32),
            pltpu.SMEM((SEQS,), jnp.int32),
            pltpu.SMEM((HEADS,), F32),
            VMEM((2, 128), jnp.int32),
            VMEM((2, 128), F32),
            VMEM((SEQS, CTX, 128), BF16),
            VMEM((SEQS, CTX, 128), BF16),
            VMEM((1024, 512), BF16),
            VMEM((1024, 128), BF16),
            VMEM((1024, 128), BF16),
            VMEM((512, 1024), BF16),
            VMEM((128, 128), F32),
            pltpu.SemaphoreType.DMA((6,)),
            pltpu.SemaphoreType.DMA((4,)),
            pltpu.SemaphoreType.DMA((8,)),
            pltpu.SemaphoreType.DMA((8,)),
        ],
        compiler_params=pltpu.CompilerParams(vmem_limit_bytes=40 * 1024 * 1024),
        cost_estimate=pl.CostEstimate(flops=2 * 10**9, bytes_accessed=11 * 2**20, transcendentals=400000),
    )(
        tokens,
        gain.reshape(1, 1024),
        lengths,
        offset,
        routes.T,
        route_weights.T,
        key_cache,
        value_cache,
        wq,
        wk,
        wv,
        wo,
    )


def expert_kernel(
    part_ref,
    tokens_ref,
    gain_ref,
    pick_ref,
    weight_ref,
    wg_hbm,
    wu_hbm,
    wd_hbm,
    out_ref,
    wg,
    wu,
    wd,
    other_part,
    outgoing,
    arrived,
    rows,
    own_sums,
    pair_send,
    pair_recv,
    up_send,
    up_recv,
    back_send,
    back_recv,
    weight_sem,
    part_sem,
    out_send_sem,
    out_recv_sem,
    ring_send_sem,
    ring_recv_sem,
    twin_send_sem,
    twin_recv_sem,
    pair_send_sem,
    pair_recv_sem,
    up_send_sem,
    up_recv_sem,
    back_send_sem,
    back_recv_sem,
):
    ep = lax.axis_index("ep")
    c = lax.axis_index("tp")
    x = ep % 4
    y = (ep // 4) % 4
    z = ep // 16

    def at(zz, yy, xx):
        return {"ep": (zz * 4 + yy) * 4 + xx, "tp": c}

    twin = {"ep": ep, "tp": 1 - c}
    right = at(z, y, (x + 1) % 4)
    left = at(z, y, (x + 3) % 4)
    across = at(z, y + 1 - 2 * (y % 2), x)

    def there(dz, f):
        return at((z + dz) % 8, (3 - y) if f else y, x)

    def back(dz, f):
        return at((z + 8 - dz) % 8, (3 - y) if f else y, x)

    far_first = [(dz, f) for dz in (4, 3, 5, 2, 6, 1, 7, 0) for f in (1, 0) if (dz, f) != (0, 0)]

    loads = [
        pltpu.make_async_copy(wg_hbm, wg, weight_sem.at[0]),
        pltpu.make_async_copy(wu_hbm, wu, weight_sem.at[1]),
        pltpu.make_async_copy(wd_hbm, wd, weight_sem.at[2]),
    ]
    for load in loads:
        load.start()

    barrier = pltpu.get_barrier_semaphore()
    for device in [there(dz, f) for dz, f in far_first] + [right, left, across, twin]:
        pl.semaphore_signal(barrier, inc=1, device_id=device, device_id_type=MESH)
    pl.semaphore_wait(barrier, 19)

    started = []

    def send(src, dst, send_sem, recv_sem, device):
        copy = pltpu.make_async_remote_copy(
            src_ref=src, dst_ref=dst, send_sem=send_sem, recv_sem=recv_sem, device_id=device, device_id_type=MESH
        )
        copy.start()
        started.append(copy)

    def arrival(dst, recv_sem):
        pltpu.make_async_remote_copy(
            src_ref=dst, dst_ref=dst, send_sem=recv_sem, recv_sem=recv_sem, device_id=twin, device_id_type=MESH
        ).wait_recv()

    send(part_ref, other_part, part_sem.at[0], part_sem.at[1], twin)
    arrival(other_part, part_sem.at[1])
    middle = tokens_ref[...].astype(F32) + (part_ref[...].astype(F32) + other_part[...].astype(F32))
    middle = middle.astype(BF16).astype(F32)
    moe_in = rms_rows(middle, gain_ref[...])
    moe_half = jnp.where(c == 0, moe_in[:, :512].astype(F32), moe_in[:, 512:].astype(F32)).astype(BF16)

    pick = pick_ref[...].astype(F32)
    half_row = (iota((128, 128), 0) // 4) % 2
    pick_wide = jnp.concatenate(
        [jnp.where(half_row == 0, pick, 0.0).astype(BF16), jnp.where(half_row == 1, pick, 0.0).astype(BF16)], axis=1
    )
    tall = jnp.concatenate([moe_half[:, :256]] * 8 + [moe_half[:, 256:]] * 8, axis=0)
    outgoing[...] = dot(pick_wide, tall).astype(BF16).reshape(16, 8, 256)
    for dz, f in far_first:
        n = 2 * dz + f
        expert = 2 * ((z + dz) % 8) + (y // 2 + f) % 2
        send(outgoing.at[expert], arrived.at[n], out_send_sem.at[n], out_recv_sem.at[n], there(dz, f))
    own_expert = 2 * z + y // 2
    arrived[0] = outgoing[own_expert]
    for dz, f in reversed(far_first):
        n = 2 * dz + f
        arrival(arrived.at[n], out_recv_sem.at[n])

    pool = arrived[...].reshape(128, 256)
    to_row = iota((64, 128), 0)
    from_row = iota((64, 128), 1)
    gather_left = (from_row == (to_row // 4) * 8 + to_row % 4).astype(F32).astype(BF16)
    gather_right = (from_row == (to_row // 4) * 8 + 4 + to_row % 4).astype(F32).astype(BF16)
    rows[0, c] = jnp.concatenate([dot(gather_left, pool), dot(gather_right, pool)], axis=1).astype(BF16)

    def pass_on(block, number, device, to_block, part=None):
        src, dst = rows.at[block, c], rows.at[to_block, c]
        if part is not None:
            src, dst = src.at[pl.ds(32 * part, 32)], dst.at[pl.ds(32 * part, 32)]
        slot = 8 if part == 1 else to_block
        send(src, dst, ring_send_sem.at[number], ring_recv_sem.at[slot], device)

    def share(block):
        send(rows.at[block, c], rows.at[block, c], twin_send_sem.at[block], twin_recv_sem.at[block], twin)

    def have(block):
        if block == 2:
            for part in range(2):
                arrival(rows.at[2, c].at[pl.ds(32 * part, 32)], ring_recv_sem.at[8 if part else 2])
        else:
            arrival(rows.at[block, c], ring_recv_sem.at[block])

    pass_on(0, 0, across, 4)
    pass_on(0, 1, right, 1)
    pass_on(0, 2, left, 3)
    share(0)
    have(4)
    pass_on(4, 3, right, 5)
    pass_on(4, 4, left, 7)
    share(4)
    have(1)
    pass_on(1, 5, right, 2, part=0)
    share(1)
    have(3)
    pass_on(3, 6, left, 2, part=1)
    share(3)

    def run(block_a, block_b):
        for block in (block_a, block_b):
            arrival(rows.at[block, 1 - c], twin_recv_sem.at[block])
        left_in = jnp.concatenate([rows[block_a, 0], rows[block_b, 0]], axis=0)
        right_in = jnp.concatenate([rows[block_a, 1], rows[block_b, 1]], axis=0)
        gate = dot_nt(left_in, wg[:, :512]) + dot_nt(right_in, wg[:, 512:])
        upward = dot_nt(left_in, wu[:, :512]) + dot_nt(right_in, wu[:, 512:])
        hidden = (gate / (1.0 + jnp.exp(-gate)) * upward).astype(BF16)
        outs = dot(hidden, wd[...])
        mine = jnp.where(c == 0, outs[:, :512], outs[:, 512:])
        theirs = jnp.where(c == 0, outs[:, 512:], outs[:, :512]).astype(BF16)
        for k, block in enumerate((block_a, block_b)):
            own_sums[block] = mine[64 * k : 64 * k + 64]
            pair_send[block] = theirs[64 * k : 64 * k + 64]
            send(pair_send.at[block], pair_recv.at[block], pair_send_sem.at[block], pair_recv_sem.at[block], twin)

    for load in loads:
        load.wait()
    run(0, 4)
    have(2)
    pass_on(2, 7, across, 6)
    share(2)
    run(1, 3)
    have(5)
    share(5)
    have(7)
    share(7)
    have(6)
    share(6)
    run(5, 7)
    run(2, 6)

    def chip_sum(block):
        arrival(pair_recv.at[block], pair_recv_sem.at[block])
        return own_sums[block] + pair_recv[block].astype(F32)

    def give(number, value, device):
        up_send[number] = value.astype(BF16)
        send(up_send.at[number], up_recv.at[number], up_send_sem.at[number], up_recv_sem.at[number], device)

    def taken(number):
        arrival(up_recv.at[number], up_recv_sem.at[number])
        return up_recv[number].astype(F32)

    give(0, chip_sum(5), left)
    give(1, chip_sum(7), right)
    give(2, chip_sum(6), across)
    far = chip_sum(2) + taken(2)
    up_send[3] = far.astype(BF16)
    for part, device in ((0, left), (1, right)):
        piece = pl.ds(32 * part, 32)
        send(
            up_send.at[3].at[piece],
            up_recv.at[3].at[piece],
            up_send_sem.at[3 + part],
            up_recv_sem.at[3 + part],
            device,
        )
    give(5, chip_sum(4) + taken(0) + taken(1), across)
    for part in range(2):
        arrival(up_recv.at[3].at[pl.ds(32 * part, 32)], up_recv_sem.at[3 + part])
    sum_1, sum_3 = chip_sum(1), chip_sum(3)
    give(6, jnp.concatenate([sum_1[:32] + up_recv[3, :32].astype(F32), sum_1[32:]], axis=0), left)
    give(7, jnp.concatenate([sum_3[:32], sum_3[32:] + up_recv[3, 32:].astype(F32)], axis=0), right)
    result = chip_sum(0) + taken(5) + taken(6) + taken(7)

    result = result.astype(BF16)
    to_pool = iota((128, 64), 0)
    from_slot = iota((128, 64), 1)
    spread = to_pool // 8 * 4 + to_pool % 4 == from_slot
    left_half = (to_pool // 4) % 2 == 0
    spread_left = jnp.logical_and(spread, left_half).astype(F32).astype(BF16)
    spread_right = jnp.logical_and(spread, jnp.logical_not(left_half)).astype(F32).astype(BF16)
    pool = dot(spread_left, result[:, :256]) + dot(spread_right, result[:, 256:])
    back_send[...] = pool.astype(BF16).reshape(16, 8, 256)
    for dz, f in far_first:
        n = 2 * dz + f
        send(back_send.at[n], back_recv.at[own_expert], back_send_sem.at[n], back_recv_sem.at[n], back(dz, f))
    back_recv[own_expert] = back_send[0]
    for dz, f in reversed(far_first):
        n = 2 * dz + f
        expert = 2 * ((z + dz) % 8) + (y // 2 + f) % 2
        arrival(back_recv.at[expert], back_recv_sem.at[n])
    pool = back_recv[...].reshape(128, 256)
    weight = weight_ref[...]
    column_half = (iota((16, 128), 1) // 4) % 2
    mixture = []
    for k in range(2):
        part = jnp.where(column_half == k, weight, 0.0)
        high = part.astype(BF16)
        mixture.append(dot(high, pool) + dot((part - high.astype(F32)).astype(BF16), pool))
    own_middle = jnp.where(c == 0, middle[:, :512], middle[:, 512:])
    out_ref[...] = (own_middle + jnp.concatenate(mixture, axis=1)).astype(BF16)
    for copy in started:
        copy.wait_send()


def experts(part, tokens, gain, pick, weight, w_gate, w_up, w_down):
    hbm = pl.BlockSpec(memory_space=HBM)
    vmem = pl.BlockSpec(memory_space=VMEM)
    dma = pltpu.SemaphoreType.DMA
    return pl.pallas_call(
        expert_kernel,
        name="experts",
        out_shape=jax.ShapeDtypeStruct((SEQS, 512), BF16),
        in_specs=[vmem] * 5 + [hbm] * 3,
        out_specs=vmem,
        scratch_shapes=[
            VMEM((448, 1024), BF16),
            VMEM((448, 1024), BF16),
            VMEM((448, 1024), BF16),
            VMEM((SEQS, 1024), BF16),
            VMEM((16, 8, 256), BF16),
            VMEM((16, 8, 256), BF16),
            VMEM((8, 2, 64, 512), BF16),
            VMEM((8, 64, 512), F32),
            VMEM((8, 64, 512), BF16),
            VMEM((8, 64, 512), BF16),
            VMEM((8, 64, 512), BF16),
            VMEM((8, 64, 512), BF16),
            VMEM((16, 8, 256), BF16),
            VMEM((16, 8, 256), BF16),
            dma((3,)),
            dma((2,)),
            dma((16,)),
            dma((16,)),
            dma((8,)),
            dma((9,)),
            dma((8,)),
            dma((8,)),
            dma((8,)),
            dma((8,)),
            dma((8,)),
            dma((8,)),
            dma((16,)),
            dma((16,)),
        ],
        compiler_params=pltpu.CompilerParams(
            collective_id=0, has_side_effects=True, vmem_limit_bytes=32 * 1024 * 1024
        ),
        cost_estimate=pl.CostEstimate(flops=2 * 10**9, bytes_accessed=3 * 2**20, transcendentals=300000),
    )(part, tokens, gain.reshape(1, 1024), pick, weight, w_gate.T, w_up.T, w_down)


def shards(
    tokens,
    lengths,
    routes,
    route_weights,
    key_cache,
    value_cache,
    w_query,
    w_key,
    w_value,
    w_out,
    score_offset,
    attn_gain,
    ffn_gain,
    w_gate,
    w_up,
    w_down,
):
    part, new_keys, new_values, pick, weight = attend(
        tokens,
        lengths,
        routes,
        route_weights,
        key_cache,
        value_cache,
        w_query,
        w_key,
        w_value,
        w_out,
        score_offset,
        attn_gain,
    )
    layer_out = experts(part, tokens, ffn_gain, pick, weight, w_gate, w_up, w_down)
    return (layer_out, new_keys, new_values)


def solution(mesh):
    in_specs = (
        P("ep", None),
        P("ep"),
        P(),
        P(),
        P("ep", None, "tp"),
        P("ep", None, "tp"),
        P(None, "tp"),
        P(None, "tp"),
        P(None, "tp"),
        P("tp", None),
        P("tp"),
        P(),
        P(),
        P(None, ("ep", "tp")),
        P(None, ("ep", "tp")),
        P(("ep", "tp"), None),
    )
    out_specs = (P("ep", "tp"), P("ep", "tp"), P("ep", "tp"))
    return jax.shard_map(shards, mesh=mesh, in_specs=in_specs, out_specs=out_specs, check_vma=False)
```

time: 119 us -> 72.5 us (0.61)
  the two profiles are of different devices: /device:TPU:1 before, /device:TPU:8 now
where the time goes in v1:
time: 72.5 us; the launch traced here: 72 us
  Pallas kernels  57.8 us (80%)
  local copies, waits for them, and re-layouts  13.5 us (19%)
    pallas_call x1, Pallas kernels, experts(): pl.pallas_call(expert_kernel, name='experts', out_shape=jax.ShapeDtypeStr...  49.1 us
    unnamed x33, local copies, waits for them, and re-layouts  13.5 us
    pallas_call x1, Pallas kernels, attend(): pl.pallas_call(attend_kernel, name='attend', out_shape=(jax.ShapeDtypeStr...  8.62 us

profile of v1, /device:TPU:8, one launch (start us, length us, event | category | flops | bytes accessed | tf_op | source)
XLA Modules:
  0.0 72.0 jit_solution(2906978478600751268)
XLA Ops:
  0.6 0.0 copy-start
  0.6 2.2 %copy-done = bf16[16,1024,128]{2,1,0:T(8,128)(2,1)S(1)} copy-done((bf16[16,1024,128]{2,1,0:T(8,128)(2,1)S(1)}, bf16[16,1024,128]{2,1,0:T(8,128)(2,1)}, u32[]{:S(2)}) %copy-start) | copy-done | bytes 4194328
  2.8 0.0 copy-start.1
  2.8 2.2 %copy-done.1 = bf16[16,1024,128]{2,1,0:T(8,128)(2,1)S(1)} copy-done((bf16[16,1024,128]{2,1,0:T(8,128)(2,1)S(1)}, bf16[16,1024,128]{2,1,0:T(8,128)(2,1)}, u32[]{:S(2)}) %copy-start.1) | copy-done | bytes 4194328
  5.0 0.0 copy-start.2
  5.0 1.2 %copy-done.2 = bf16[1024,512]{1,0:T(8,128)(2,1)S(1)} copy-done((bf16[1024,512]{1,0:T(8,128)(2,1)S(1)}, bf16[1024,512]{1,0:T(8,128)(2,1)}, u32[]{:S(2)}) %copy-start.2) | copy-done | bytes 1048600
  6.2 0.0 copy-start.3
  6.2 1.2 %copy-done.3 = bf16[512,1024]{1,0:T(8,128)(2,1)S(1)} copy-done((bf16[512,1024]{1,0:T(8,128)(2,1)S(1)}, bf16[512,1024]{1,0:T(8,128)(2,1)}, u32[]{:S(2)}) %copy-start.3) | copy-done | bytes 1048600
  7.5 0.0 copy-start.4
  7.5 0.9 %copy-done.4 = bf16[1024,128]{1,0:T(8,128)(2,1)S(1)} copy-done((bf16[1024,128]{1,0:T(8,128)(2,1)S(1)}, bf16[1024,128]{1,0:T(8,128)(2,1)}, u32[]{:S(2)}) %copy-start.4) | copy-done | bytes 262168
  8.4 0.0 copy-start.5
  8.4 0.9 %copy-done.5 = bf16[1024,128]{1,0:T(8,128)(2,1)S(1)} copy-done((bf16[1024,128]{1,0:T(8,128)(2,1)S(1)}, bf16[1024,128]{1,0:T(8,128)(2,1)}, u32[]{:S(2)}) %copy-start.5) | copy-done | bytes 262168
  9.4 0.0 copy-start.6
  9.4 0.8 %copy-done.6 = bf16[16,1024]{1,0:T(8,128)(2,1)S(1)} copy-done((bf16[16,1024]{1,0:T(8,128)(2,1)S(1)}, bf16[16,1024]{1,0:T(8,128)(2,1)}, u32[]{:S(2)}) %copy-start.6) | copy-done | bytes 32792
  10.1 0.0 copy-start.7
  10.1 0.7 copy-done.7
  10.8 0.0 copy-start.8
  10.8 0.7 copy-done.8
  11.6 0.0 copy-start.9
  11.6 0.7 copy-done.9
  12.2 0.0 copy-start.10
  12.2 0.7 copy-done.10
  12.9 0.0 copy-start.11
  12.9 0.7 copy-done.11
  13.6 0.0 copy-start.12
  13.6 0.0 copy-start.13
  13.6 0.0 copy-start.14
  13.6 0.0 copy-start.15
  13.6 8.6 %attend.1 = (bf16[16,1024]{1,0:T(8,128)(2,1)S(1)}, bf16[16,128]{1,0:T(8,128)(2,1)}, bf16[16,128]{1,0:T(8,128)(2,1)}, bf16[128,128]{1,0:T(8,128)(2,1)S(1)}, f32[16,128]{1,0:T(8,128)S(1)}) custom-call(bf16[16,1024]{1,0:T(8,128)(2,1)S(1)} %copy-done.6, f32[1,1024]{1,0:T(1,128)S(1)} %bitcast.8, s32[16]{0:T(128)S(1)} %copy-done.10, f32[8]{0:T(128)S(1)} %copy-done.11, ...), custom_call_target="tpu_custom_call" | custom-call | flops 2000000000 | bytes 11534336 | tf_op jit(solution)/shard_map/attend/pallas_call | solution.py:203
  22.2 0.0 copy-done.12
  22.2 0.0 copy-done.13
  22.2 0.0 copy-done.14
  22.2 0.0 copy-done.15
  22.2 49.1 %experts.1 = bf16[16,512]{1,0:T(8,128)(2,1)S(1)} custom-call(bf16[16,1024]{1,0:T(8,128)(2,1)S(1)} %get-tuple-element.8.part_ref, bf16[16,1024]{1,0:T(8,128)(2,1)S(1)} %copy-done.6, f32[1,1024]{1,0:T(1,128)S(1)} %bitcast.11, bf16[128,128]{1,0:T(8,128)(2,1)S(1)} %get-tuple-element.9.pick_ref, f32[16,128]{1,0:T(8,128)S(1)} %get-tuple-element.10.weight_ref, ...), custom_call_target="tpu_custom_call" | custom-call | flops 2000000000 | bytes 3145728 | tf_op jit(solution)/shard_map/experts/pallas_call | solution.py:504
  71.4 0.6 copy.20
Async XLA Ops:
  0.6 2.2 %copy-start = (bf16[16,1024,128]{2,1,0:T(8,128)(2,1)S(1)}, bf16[16,1024,128]{2,1,0:T(8,128)(2,1)}, u32[]{:S(2)}) copy-start(bf16[16,1024,128]{2,1,0:T(8,128)(2,1)} %keys_hbm.1) | copy-start | bytes 12582916
  2.8 2.2 %copy-start.1 = (bf16[16,1024,128]{2,1,0:T(8,128)(2,1)S(1)}, bf16[16,1024,128]{2,1,0:T(8,128)(2,1)}, u32[]{:S(2)}) copy-start(bf16[16,1024,128]{2,1,0:T(8,128)(2,1)} %values_hbm.1) | copy-start | bytes 12582916
  5.0 1.2 %copy-start.2 = (bf16[1024,512]{1,0:T(8,128)(2,1)S(1)}, bf16[1024,512]{1,0:T(8,128)(2,1)}, u32[]{:S(2)}) copy-start(bf16[1024,512]{1,0:T(8,128)(2,1)} %wq_hbm.1) | copy-start | bytes 3145732
  6.2 1.2 %copy-start.3 = (bf16[512,1024]{1,0:T(8,128)(2,1)S(1)}, bf16[512,1024]{1,0:T(8,128)(2,1)}, u32[]{:S(2)}) copy-start(bf16[512,1024]{1,0:T(8,128)(2,1)} %wo_hbm.1) | copy-start | bytes 3145732
  7.5 0.9 %copy-start.4 = (bf16[1024,128]{1,0:T(8,128)(2,1)S(1)}, bf16[1024,128]{1,0:T(8,128)(2,1)}, u32[]{:S(2)}) copy-start(bf16[1024,128]{1,0:T(8,128)(2,1)} %wk_hbm.1) | copy-start | bytes 786436
  8.4 0.9 %copy-start.5 = (bf16[1024,128]{1,0:T(8,128)(2,1)S(1)}, bf16[1024,128]{1,0:T(8,128)(2,1)}, u32[]{:S(2)}) copy-start(bf16[1024,128]{1,0:T(8,128)(2,1)} %wv_hbm.1) | copy-start | bytes 786436
  9.4 0.8 %copy-start.6 = (bf16[16,1024]{1,0:T(8,128)(2,1)S(1)}, bf16[16,1024]{1,0:T(8,128)(2,1)}, u32[]{:S(2)}) copy-start(bf16[16,1024]{1,0:T(8,128)(2,1)} %tokens_ref.1) | copy-start | bytes 98308
  10.1 0.7 copy-start.7
  10.8 0.7 copy-start.8
  11.6 0.7 copy-start.9
  12.2 0.7 copy-start.10
  12.9 0.7 copy-start.11
  13.6 8.6 %copy-start.12 = (bf16[1024,448]{0,1:T(8,128)(2,1)S(1)}, bf16[1024,448]{0,1:T(8,128)(2,1)}, u32[]{:S(2)}) copy-start(bf16[1024,448]{0,1:T(8,128)(2,1)} %param.29) | copy-start | bytes 2752516
  13.6 8.6 %copy-start.13 = (bf16[1024,448]{0,1:T(8,128)(2,1)S(1)}, bf16[1024,448]{0,1:T(8,128)(2,1)}, u32[]{:S(2)}) copy-start(bf16[1024,448]{0,1:T(8,128)(2,1)} %param.30) | copy-start | bytes 2752516
  13.6 8.7 %copy-start.14 = (bf16[448,1024]{1,0:T(8,128)(2,1)S(1)}, bf16[448,1024]{1,0:T(8,128)(2,1)}, u32[]{:S(2)}) copy-start(bf16[448,1024]{1,0:T(8,128)(2,1)} %wd_hbm.1) | copy-start | bytes 2752516
  13.6 8.7 %copy-start.15 = (f32[1024]{0:T(1024)S(1)}, f32[1024]{0:T(1024)}, u32[]{:S(2)}) copy-start(f32[1024]{0:T(1024)} %param.28) | copy-start | bytes 12292
